TPU v7x, 32 devices: a whole 2x2x4 slice. The times are simulated.
32 devices in a mesh: sp: 4 (over z), fs: 4 (over y, x), tp: 2 (over core).
Axes of the slice: x: 2, y: 2, z: 4, core: 2. Of those that a mesh axis runs over, the one named last changes fastest.
Arguments:
- tokens: bfloat16 [4, 8192, 2048], P('fs', 'sp'), may hold values from -21 to 21
- norm_gain: float32 [2048], replicated, may hold values from 0.1 to 1.9
- w_query: bfloat16 [2048, 1024], P(None, 'tp'), may hold values from -0.125 to 0.125
- w_key: bfloat16 [2048, 256], P(None, 'tp'), may hold values from -0.125 to 0.125
- w_value: bfloat16 [2048, 256], P(None, 'tp'), may hold values from -0.125 to 0.125
- w_pool: bfloat16 [2048, 1024], P(None, 'tp'), may hold values from -0.125 to 0.125
- w_group: bfloat16 [4, 256, 256], P('tp'), may hold values from -0.375 to 0.375
- w_out: bfloat16 [2048, 2048], replicated, may hold values from -0.125 to 0.125
- sinks: float32 [16], P('tp'), may hold values from -1 to 260
Outputs:
- mixed: bfloat16 [4, 8192, 2048], P('fs', ('sp', 'tp'))
- log_sums: float32 [4, 16, 8192], P('fs', 'tp', 'sp')
All inputs are finite; a program needn't handle non-finite values.
Results may differ from a plain program's by a relative error of at most 0.009.
Values may be sent and summed in bfloat16 or wider, within the bound.
No kernel may reach another device: no remote copies, remote signals or barrier semaphores. Data moves between devices by JAX's collectives and lax.ppermute only.
A program may use at most 192 MiB of HBM per device.

v0:
```python
import jax
import jax.numpy as jnp
from jax import lax
from jax.experimental import pallas as pl
from jax.experimental.pallas import tpu as pltpu
from jax.sharding import PartitionSpec as P

HEAD_SIZE = 64
GROUPS = 4
GDIM = 256
WINDOW_KEYS = 128
LN_EPS = 1e-05

ROWS = 512
TILE = 256
REACH = 16
F32 = jnp.float32
BF16 = jnp.bfloat16


def dot(a, b, dims=((1,), (0,))):
    return lax.dot_general(a, b, (dims, ((), ())), preferred_element_type=F32)


def project_kernel(x_ref, gain_ref, wk_ref, wv_ref, wp_ref, n_ref, kv_ref, p_ref, sums_ref,
                   tail_ref, tot_ref, wkv, total):
    step = pl.program_id(0)
    last = pl.num_programs(0) - 1
    kw = wk_ref.shape[1]
    pw = wp_ref.shape[1]

    @pl.when(step == 0)
    def _():
        wkv[:, :kw] = wk_ref[...]
        wkv[:, kw:] = wv_ref[...]
        total[...] = jnp.zeros_like(total)

    rows = x_ref.shape[0]
    gain = gain_ref[...]
    running = total[0:1]
    for part in range(rows // TILE):
        span = slice(part * TILE, (part + 1) * TILE)
        x = x_ref[span].astype(F32)
        centered = x - jnp.mean(x, axis=-1, keepdims=True)
        variance = jnp.mean(centered * centered, axis=-1, keepdims=True)
        normed = (centered * lax.rsqrt(variance + LN_EPS) * gain).astype(BF16)
        n_ref[span] = normed
        kv_ref[span] = dot(normed, wkv[...]).astype(BF16)
        pool = dot(normed, wp_ref[...]).astype(BF16)
        p_ref[span] = pool
        part_sum = jnp.sum(pool.astype(F32), axis=0, keepdims=True)
        sums_ref[pl.ds(step * (rows // TILE) + part, 1)] = part_sum
        running = running + part_sum
    total[0:1] = running

    @pl.when(step == last)
    def _():
        hi = running.astype(BF16).astype(F32)
        mid = (running - hi).astype(BF16).astype(F32)
        low = running - hi - mid
        tot = jnp.concatenate([hi, mid, low, jnp.zeros((REACH - 3, pw), F32)], axis=0).astype(BF16)
        tot_ref[...] = tot
        tail_ref[...] = jnp.zeros_like(tail_ref)
        tail_ref[:WINDOW_KEYS, : 2 * kw] = kv_ref[rows - WINDOW_KEYS :]
        tail_ref[WINDOW_KEYS : WINDOW_KEYS + REACH] = p_ref[rows - REACH :]
        tail_ref[WINDOW_KEYS + REACH :] = tot


def project(x, gain, wk, wv, wp):
    length, d = x.shape
    kw, pw = wk.shape[1], wp.shape[1]
    rows = min(ROWS, length)
    whole = lambda shape: pl.BlockSpec(shape, lambda i: (0, 0))
    tail_rows = WINDOW_KEYS + 2 * REACH
    return pl.pallas_call(
        project_kernel,
        name="project",
        grid=(length // rows,),
        in_specs=[
            pl.BlockSpec((rows, d), lambda i: (i, 0)),
            whole((1, d)),
            whole((d, kw)),
            whole((d, kw)),
            whole((d, pw)),
        ],
        out_specs=[
            pl.BlockSpec((rows, d), lambda i: (i, 0)),
            pl.BlockSpec((rows, 2 * kw), lambda i: (i, 0)),
            pl.BlockSpec((rows, pw), lambda i: (i, 0)),
            whole((length // TILE, pw)),
            whole((tail_rows, pw)),
            whole((REACH, pw)),
        ],
        out_shape=[
            jax.ShapeDtypeStruct((length, d), BF16),
            jax.ShapeDtypeStruct((length, 2 * kw), BF16),
            jax.ShapeDtypeStruct((length, pw), BF16),
            jax.ShapeDtypeStruct((length // TILE, pw), F32),
            jax.ShapeDtypeStruct((tail_rows, pw), BF16),
            jax.ShapeDtypeStruct((REACH, pw), BF16),
        ],
        scratch_shapes=[pltpu.VMEM((d, 2 * kw), BF16), pltpu.VMEM((8, pw), F32)],
        cost_estimate=pl.CostEstimate(
            flops=2 * length * d * (2 * kw + pw), bytes_accessed=6 * length * d, transcendentals=0
        ),
        compiler_params=pltpu.CompilerParams(dimension_semantics=("arbitrary",)),
    )(x, gain, wk, wv, wp)


def query_kernel(n_ref, w_ref, q_ref):
    q_ref[...] = (dot(n_ref[...], w_ref[...]) * HEAD_SIZE ** (-0.5)).astype(BF16)


def project_queries(normed, wq):
    length, d = normed.shape
    qw = wq.shape[1]
    rows = min(ROWS, length)
    return pl.pallas_call(
        query_kernel,
        name="queries",
        grid=(length // rows,),
        in_specs=[
            pl.BlockSpec((rows, d), lambda i: (i, 0)),
            pl.BlockSpec((d, qw), lambda i: (0, 0)),
        ],
        out_specs=pl.BlockSpec((rows, qw), lambda i: (i, 0)),
        out_shape=jax.ShapeDtypeStruct((length, qw), BF16),
        cost_estimate=pl.CostEstimate(
            flops=2 * length * d * qw, bytes_accessed=2 * length * d, transcendentals=0
        ),
        compiler_params=pltpu.CompilerParams(dimension_semantics=("arbitrary",)),
    )(normed, wq)


def mixer_kernel(further, where_ref, q_ref, kv_ref, kvp_ref, p_ref, pp_ref, sums_ref, tail_ref,
                 *refs):
    tots = refs[:further]
    wg_ref, sink_ref, _, act_ref, log_ref = refs[further:]
    seq_part = where_ref[1]
    tile = where_ref[0] * pl.num_programs(0) + pl.program_id(0)
    first = tile == 0
    rows, qw = q_ref.shape
    kw = kv_ref.shape[1] // 2
    pw = p_ref.shape[1]
    length = sums_ref.shape[0] * rows

    x = p_ref[...]
    row = lax.broadcasted_iota(jnp.int32, (rows, rows), 0)
    col = lax.broadcasted_iota(jnp.int32, (rows, rows), 1)
    gap = row - col
    lower = jnp.where(gap >= 0, 1.0, 0.0).astype(BF16)
    before = lax.broadcasted_iota(jnp.int32, sums_ref.shape, 0) < tile
    carry = jnp.sum(jnp.where(before, sums_ref[...], 0.0), axis=0, keepdims=True)
    for got in (tail_ref[WINDOW_KEYS + REACH :],) + tuple(t[...] for t in tots):
        carry = carry + jnp.sum(got.astype(F32), axis=0, keepdims=True)
    prev_pool = jnp.where(
        first, tail_ref[WINDOW_KEYS : WINDOW_KEYS + REACH].astype(F32), pp_ref[...].astype(F32)
    ).astype(BF16)
    spot = seq_part * length + tile * rows + lax.broadcasted_iota(jnp.int32, (rows, 1), 0) + 1
    inverse_spot = 1.0 / spot.astype(F32)
    edge_gap = (
        lax.broadcasted_iota(jnp.int32, (REACH, REACH), 0)
        + REACH
        - lax.broadcasted_iota(jnp.int32, (REACH, REACH), 1)
    )
    for slot in range(pw // GDIM):
        lanes = slice(slot * GDIM, (slot + 1) * GDIM)
        width = jnp.left_shift(jnp.int32(2), where_ref[2] * (pw // GDIM) + slot)
        band = jnp.where((gap >= 0) & (gap < width), 1.0, 0.0).astype(BF16)
        edge = jnp.where(edge_gap < width, 1.0, 0.0).astype(BF16)
        window = dot(band, x[:, lanes])
        window = jnp.concatenate(
            [window[:REACH] + dot(edge, prev_pool[:, lanes]), window[REACH:]], axis=0
        )
        prefix = dot(lower, x[:, lanes]) + carry[:, lanes]
        inverse_count = 1.0 / jnp.minimum(spot, width).astype(F32)
        pooled = (window * inverse_count - prefix * inverse_spot).astype(BF16)
        act_ref[:, lanes] = dot(pooled, wg_ref[slot]).astype(BF16)

    wk = WINDOW_KEYS
    key = lax.broadcasted_iota(jnp.int32, (wk, wk), 0)
    query = lax.broadcasted_iota(jnp.int32, (wk, wk), 1)
    is_prev = key > query
    prev_one = jnp.where(is_prev, 1.0, 0.0).astype(BF16)
    own_one = jnp.where(is_prev, 0.0, 1.0).astype(BF16)
    kv_prev = jnp.where(
        first, tail_ref[:wk, : 2 * kw].astype(F32), kvp_ref[...].astype(F32)
    ).astype(BF16)
    no_prev = jnp.where(first & (seq_part == 0), -1e30, 0.0).astype(F32)
    kv_count = kw // HEAD_SIZE
    pairs = qw // HEAD_SIZE // kv_count // 2
    two = 2 * HEAD_SIZE
    for block in range(rows // wk):
        span = slice(block * wk, (block + 1) * wk)
        own = kv_ref[span]
        both = jnp.concatenate([kv_prev, own], axis=0)
        keys = both[:, :kw]
        values_t = both[:, kw:].astype(F32).T.astype(BF16)
        for kv_head in range(kv_count):
            head_key = keys[:, kv_head * HEAD_SIZE : (kv_head + 1) * HEAD_SIZE]
            blank = jnp.zeros_like(head_key)
            stacked = jnp.concatenate(
                [
                    jnp.concatenate([head_key, blank], axis=1),
                    jnp.concatenate([blank, head_key], axis=1),
                ],
                axis=0,
            )
            base = kv_head * pairs
            queries = jnp.concatenate(
                [q_ref[span, (base + p) * two : (base + p + 1) * two] for p in range(pairs)], axis=0
            )
            scores = dot(stacked, queries, ((1,), (1,)))
            head_values = values_t[kv_head * HEAD_SIZE : (kv_head + 1) * HEAD_SIZE]
            halves = []
            for odd in range(2):
                columns = []
                scales = []
                for p in range(pairs):
                    head = (base + p) * 2 + odd
                    cols = slice(p * wk, (p + 1) * wk)
                    seen = jnp.where(
                        is_prev,
                        scores[odd * 2 * wk : odd * 2 * wk + wk, cols] + no_prev
                        if block == 0
                        else scores[odd * 2 * wk : odd * 2 * wk + wk, cols],
                        scores[odd * 2 * wk + wk : (odd + 1) * 2 * wk, cols],
                    )
                    sink = sink_ref[head]
                    row_max = jnp.maximum(jnp.max(seen, axis=0, keepdims=True), sink)
                    weights = jnp.exp(seen - row_max)
                    weight_sum = jnp.sum(weights, axis=0, keepdims=True) + jnp.exp(sink - row_max)
                    log_ref[head : head + 1, span] = row_max + jnp.log(weight_sum)
                    weights = weights.astype(BF16)
                    columns.append(
                        jnp.concatenate([weights * prev_one, weights * own_one], axis=0)
                    )
                    scales.append(1.0 / weight_sum)
                out = dot(head_values, jnp.concatenate(columns, axis=1))
                halves.append(out * jnp.concatenate(scales, axis=1))
            for p in range(pairs):
                cols = slice(p * wk, (p + 1) * wk)
                pair = jnp.concatenate([halves[0][:, cols], halves[1][:, cols]], axis=0).T
                first_lane = pw + (base + p) * two
                act_ref[span, first_lane : first_lane + two] = pair.astype(BF16)
        kv_prev = own


def mix(where, q, kv, pool, sums, tail, tots, w_group, sinks, logs, steps):
    length, qw = q.shape
    kw2, pw = kv.shape[1], pool.shape[1]
    tile = lambda i, w: w[0] * steps + i
    spec = pl.BlockSpec
    heads = qw // HEAD_SIZE
    in_specs = [
        spec((TILE, qw), lambda i, w: (tile(i, w), 0)),
        spec((TILE, kw2), lambda i, w: (tile(i, w), 0)),
        spec((WINDOW_KEYS, kw2), lambda i, w: (jnp.maximum(tile(i, w) * (TILE // WINDOW_KEYS) - 1, 0), 0)),
        spec((TILE, pw), lambda i, w: (tile(i, w), 0)),
        spec((REACH, pw), lambda i, w: (jnp.maximum(tile(i, w) * (TILE // REACH) - 1, 0), 0)),
        spec(sums.shape, lambda i, w: (0, 0)),
        spec(tail.shape, lambda i, w: (0, 0)),
    ]
    in_specs += [spec(t.shape, lambda i, w: (0, 0)) for t in tots]
    in_specs += [
        spec(w_group.shape, lambda i, w: (0, 0, 0)),
        spec(memory_space=pltpu.SMEM),
        spec(memory_space=pl.ANY),
    ]
    operands = (where, q, kv, kv, pool, pool, sums, tail, *tots, w_group, sinks, logs)
    return pl.pallas_call(
        lambda *refs: mixer_kernel(len(tots), *refs),
        name="mixer",
        grid_spec=pltpu.PrefetchScalarGridSpec(
            num_scalar_prefetch=1,
            grid=(steps,),
            in_specs=in_specs,
            out_specs=[
                spec((TILE, pw + qw), lambda i, w: (i, 0)),
                spec((heads, TILE), lambda i, w: (0, tile(i, w))),
            ],
        ),
        out_shape=[
            jax.ShapeDtypeStruct((steps * TILE, pw + qw), BF16),
            jax.ShapeDtypeStruct((heads, length), F32),
        ],
        input_output_aliases={len(operands) - 1: 1},
        cost_estimate=pl.CostEstimate(
            flops=8 * steps * TILE * (WINDOW_KEYS * qw + TILE * pw),
            bytes_accessed=6 * steps * TILE * (pw + qw),
            transcendentals=0,
        ),
        compiler_params=pltpu.CompilerParams(dimension_semantics=("arbitrary",)),
    )(*operands)


def output_kernel(where_ref, a_ref, b_ref, wa0, wa1, wb0, wb1, o_ref):
    half = wa0.shape[1]
    total = dot(a_ref[:, :half], wa0[0]) + dot(a_ref[:, half:], wa1[0])
    total = total + dot(b_ref[:, :half], wb0[0]) + dot(b_ref[:, half:], wb1[0])
    o_ref[...] = total.astype(BF16)


def project_out(where, own, other, w_out, width):
    rows, inner = own.shape
    d = w_out.shape[1]
    chunk = inner // 2
    blocks = w_out.reshape(w_out.shape[0] // chunk, chunk, d)
    spec = pl.BlockSpec
    weight = lambda place: spec((1, chunk, width), lambda j, w: (place(w[2]), 0, j))
    return pl.pallas_call(
        output_kernel,
        name="output",
        grid_spec=pltpu.PrefetchScalarGridSpec(
            num_scalar_prefetch=1,
            grid=(d // width,),
            in_specs=[
                spec((rows, inner), lambda j, w: (0, 0)),
                spec((rows, inner), lambda j, w: (0, 0)),
                weight(lambda t: t),
                weight(lambda t: 2 + t),
                weight(lambda t: 1 - t),
                weight(lambda t: 3 - t),
            ],
            out_specs=spec((rows, width), lambda j, w: (0, j)),
        ),
        out_shape=jax.ShapeDtypeStruct((rows, d), BF16),
        cost_estimate=pl.CostEstimate(
            flops=4 * rows * inner * d, bytes_accessed=6 * rows * d, transcendentals=0
        ),
        compiler_params=pltpu.CompilerParams(dimension_semantics=("arbitrary",)),
    )(where, own, other, blocks, blocks, blocks, blocks)


def body(tokens, norm_gain, w_query, w_key, w_value, w_pool, w_group, w_out, sinks):
    x = tokens[0]
    length = x.shape[0]
    parts = lax.axis_size("sp")
    sp, tp = lax.axis_index("sp"), lax.axis_index("tp")
    normed, kv, pool, sums, tail, tot = project(x, norm_gain[None, :], w_key, w_value, w_pool)
    ahead = lambda value, steps: lax.ppermute(
        value, "sp", [(source, source + steps) for source in range(parts - steps)]
    )
    tail = ahead(tail, 1)
    tots = [ahead(tot, steps) for steps in range(2, parts)]
    q = project_queries(normed, w_query)
    steps = length // TILE // 2
    heads = q.shape[1] // HEAD_SIZE
    place = lambda half: jnp.stack([half, sp, tp]).astype(jnp.int32)
    logs = jnp.zeros((heads, length), F32)
    sent, logs = mix(place(1 - tp), q, kv, pool, sums, tail, tots, w_group, sinks, logs, steps)
    other = lax.ppermute(sent, "tp", [(0, 1), (1, 0)])
    own, logs = mix(place(tp), q, kv, pool, sums, tail, tots, w_group, sinks, logs, steps)
    mixed = project_out(place(tp), own, other, w_out, 512)
    return (mixed[None], logs[None])


def solution(mesh):
    return jax.shard_map(
        body,
        mesh=mesh,
        in_specs=(
            P("fs", "sp", None),
            P(),
            P(None, "tp"),
            P(None, "tp"),
            P(None, "tp"),
            P(None, "tp"),
            P("tp", None, None),
            P(),
            P("tp"),
        ),
        out_specs=(P("fs", ("sp", "tp"), None), P("fs", "tp", "sp")),
        check_vma=False,
    )
```

profile of v0, /device:TPU:1, one launch (start us, length us, event | category | flops | bytes accessed | tf_op | source)
XLA Modules:
  0.0 74.2 jit_solution(10785910937275902427)
XLA Ops:
  0.6 15.1 %project.1 = (bf16[2048,2048]{1,0:T(8,128)(2,1)}, bf16[2048,256]{1,0:T(8,128)(2,1)}, bf16[2048,512]{1,0:T(8,128)(2,1)}, f32[8,512]{1,0:T(8,128)}, bf16[160,512]{1,0:T(8,128)(2,1)}, /*index=5*/bf16[16,512]{1,0:T(8,128)(2,1)}) custom-call(bf16[2048,2048]{1,0:T(8,128)(2,1)} %bitcast.14, f32[1,2048]{1,0:T(1,128)} %bitcast.15, bf16[2048,128]{1,0:T(8,128)(2,1)} %wk_ref.1, ...), custom_call_target="tpu_custom_call" | custom-call | flops 6442450944 | bytes 25165824 | tf_op jit(solution)/shard_map/project/pallas_call | solution.py:75
  15.7 5.0 %collective-permute-start.1 = (bf16[16,512]{1,0:T(8,128)(2,1)}, bf16[16,512]{1,0:T(8,128)(2,1)S(1)}, u32[]{:S(2)}, u32[]{:S(2)}) collective-permute-start(bf16[16,512]{1,0:T(8,128)(2,1)} %get-tuple-element.17), channel_id=1, source_target_pairs={{0,16},{8,24},{1,17},{9,25},{2,18},{10,26},{3,19},{11,27},{4,20},{... | collective-permute-start | bytes 49160 | tf_op jit(solution)/shard_map/ppermute | solution.py:341
  20.8 2.3 %collective-permute-start.2 = (bf16[16,512]{1,0:T(8,128)(2,1)}, bf16[16,512]{1,0:T(8,128)(2,1)S(1)}, u32[]{:S(2)}, u32[]{:S(2)}) collective-permute-start(bf16[16,512]{1,0:T(8,128)(2,1)} %get-tuple-element.17), channel_id=1, source_target_pairs={{0,24},{1,25},{2,26},{3,27},{4,28},{5,29},{6,30},{7,31}} | collective-permute-start | bytes 49160 | tf_op jit(solution)/shard_map/ppermute | solution.py:341
  23.1 1.6 %collective-permute-start = (bf16[160,512]{1,0:T(8,128)(2,1)}, bf16[160,512]{1,0:T(8,128)(2,1)S(1)}, u32[]{:S(2)}, u32[]{:S(2)}) collective-permute-start(bf16[160,512]{1,0:T(8,128)(2,1)} %get-tuple-element.16), channel_id=1, source_target_pairs={{0,8},{8,16},{16,24},{1,9},{9,17},{17,25},{2,10},{10,18},{18,26},{... | collective-permute-start | bytes 491528 | tf_op jit(solution)/shard_map/ppermute | solution.py:341
  24.6 8.7 %queries.1.refs_1_ = bf16[2048,512]{1,0:T(8,128)(2,1)} custom-call(bf16[2048,2048]{1,0:T(8,128)(2,1)} %get-tuple-element.12.n_ref, bf16[2048,512]{1,0:T(8,128)(2,1)} %w_ref.1), custom_call_target="tpu_custom_call" | custom-call | flops 4294967296 | bytes 8388608 | tf_op jit(solution)/shard_map/queries/pallas_call | solution.py:118
  33.4 0.6 add_add_fusion.1.refs_0_
  33.9 0.0 collective-permute-done.1.refs_8_
  33.9 0.0 copy-start.2
  33.9 0.0 collective-permute-done.2.refs_9_
  33.9 0.0 copy-start.3
  33.9 0.0 collective-permute-done.refs_7_
  33.9 0.0 copy-start.1
  34.0 0.7 broadcast_in_dim.13.refs_12_
  34.6 0.0 copy-done.2
  34.6 0.0 copy-done.3
  34.6 0.0 copy-done.1
  34.6 11.0 %mixer.2 = (bf16[1024,1024]{1,0:T(8,128)(2,1)}, f32[8,2048]{1,0:T(8,128)}) custom-call(s32[3]{0:T(128)} %add_add_fusion.1.refs_0_, bf16[2048,512]{1,0:T(8,128)(2,1)} %queries.1.refs_1_, bf16[2048,256]{1,0:T(8,128)(2,1)} %get-tuple-element.13.refs_2_.refs_3_, bf16[2048,256]{1,0:T(8,128)(2,1)} %get-tuple-element.13.refs_2_.refs_3_, ...), custom_call_target="tpu_custom_call", output_to_operand_aliasing={{1}: (12, {})} | custom-call | flops 1610612736 | bytes 6291456 | tf_op jit(solution)/shard_map/mixer/pallas_call | solution.py:271
  45.7 1.3 %collective-permute-start.3 = (bf16[1024,1024]{1,0:T(8,128)(2,1)}, bf16[1024,1024]{1,0:T(8,128)(2,1)S(1)}, u32[]{:S(2)}, u32[]{:S(2)}) collective-permute-start(bf16[1024,1024]{1,0:T(8,128)(2,1)} %get-tuple-element.20), channel_id=1, source_target_pairs={{0,1},{1,0},{2,3},{3,2},{4,5},{5,4},{6,7},{7,6},{8,9},{9,8},{10,11... | collective-permute-start | bytes 6291464 | tf_op jit(solution)/shard_map/ppermute | solution.py:352
  47.0 0.6 add_add_fusion.refs_0_.where_ref
  47.6 11.0 %mixer.3 = (bf16[1024,1024]{1,0:T(8,128)(2,1)}, f32[8,2048]{1,0:T(8,128)}) custom-call(s32[3]{0:T(128)} %add_add_fusion.refs_0_.where_ref, bf16[2048,512]{1,0:T(8,128)(2,1)} %queries.1.refs_1_, bf16[2048,256]{1,0:T(8,128)(2,1)} %get-tuple-element.13.refs_2_.refs_3_, ...), custom_call_target="tpu_custom_call", output_to_operand_aliasing={{1}: (12, {})} | custom-call | flops 1610612736 | bytes 6291456 | tf_op jit(solution)/shard_map/mixer/pallas_call | solution.py:271
  58.6 0.0 collective-permute-done.3.b_ref
  58.7 0.0 copy-start
  58.7 1.3 %copy-done = bf16[1024,1024]{1,0:T(8,128)(2,1)} copy-done((bf16[1024,1024]{1,0:T(8,128)(2,1)}, bf16[1024,1024]{1,0:T(8,128)(2,1)S(1)}, u32[]{:S(2)}) %copy-start) | copy-done | bytes 2097176
  60.0 14.2 %output.1 = bf16[1024,2048]{1,0:T(8,128)(2,1)} custom-call(s32[3]{0:T(128)} %add_add_fusion.refs_0_.where_ref, bf16[1024,1024]{1,0:T(8,128)(2,1)} %get-tuple-element.19.a_ref, bf16[1024,1024]{1,0:T(8,128)(2,1)} %copy-done, bf16[4,512,2048]{2,1,0:T(8,128)(2,1)} %bitcast.8, bf16[4,512,2048]{2,1,0:T(8,128)(2,1)} %bitcast.9, bf16[4,512,2048]{2,1,0:T(8,128)(2,1)} %bitcast.10, ...), custom_call_target="tpu_custom_call" | custom-call | flops 8589934592 | bytes 12582912 | tf_op jit(solution)/shard_map/output/pallas_call | solution.py:311
Async XLA Ops:
  15.7 18.2 %collective-permute-start.1 = (bf16[16,512]{1,0:T(8,128)(2,1)}, bf16[16,512]{1,0:T(8,128)(2,1)S(1)}, u32[]{:S(2)}, u32[]{:S(2)}) collective-permute-start(bf16[16,512]{1,0:T(8,128)(2,1)} %get-tuple-element.17), channel_id=1, source_target_pairs={{0,16},{8,24},{1,17},{9,25},{2,18},{10,26},{3,19},{11,27},{4,20},{... | collective-permute-start | bytes 49160 | tf_op jit(solution)/shard_map/ppermute | solution.py:341
  20.8 13.2 %collective-permute-start.2 = (bf16[16,512]{1,0:T(8,128)(2,1)}, bf16[16,512]{1,0:T(8,128)(2,1)S(1)}, u32[]{:S(2)}, u32[]{:S(2)}) collective-permute-start(bf16[16,512]{1,0:T(8,128)(2,1)} %get-tuple-element.17), channel_id=1, source_target_pairs={{0,24},{1,25},{2,26},{3,27},{4,28},{5,29},{6,30},{7,31}} | collective-permute-start | bytes 49160 | tf_op jit(solution)/shard_map/ppermute | solution.py:341
  23.1 10.9 %collective-permute-start = (bf16[160,512]{1,0:T(8,128)(2,1)}, bf16[160,512]{1,0:T(8,128)(2,1)S(1)}, u32[]{:S(2)}, u32[]{:S(2)}) collective-permute-start(bf16[160,512]{1,0:T(8,128)(2,1)} %get-tuple-element.16), channel_id=1, source_target_pairs={{0,8},{8,16},{16,24},{1,9},{9,17},{17,25},{2,10},{10,18},{18,26},{... | collective-permute-start | bytes 491528 | tf_op jit(solution)/shard_map/ppermute | solution.py:341
  33.9 0.7 copy-start.2
  33.9 0.7 copy-start.3
  33.9 0.7 copy-start.1
  45.7 13.0 %collective-permute-start.3 = (bf16[1024,1024]{1,0:T(8,128)(2,1)}, bf16[1024,1024]{1,0:T(8,128)(2,1)S(1)}, u32[]{:S(2)}, u32[]{:S(2)}) collective-permute-start(bf16[1024,1024]{1,0:T(8,128)(2,1)} %get-tuple-element.20), channel_id=1, source_target_pairs={{0,1},{1,0},{2,3},{3,2},{4,5},{5,4},{6,7},{7,6},{8,9},{9,8},{10,11... | collective-permute-start | bytes 6291464 | tf_op jit(solution)/shard_map/ppermute | solution.py:352
  58.7 1.3 %copy-start = (bf16[1024,1024]{1,0:T(8,128)(2,1)}, bf16[1024,1024]{1,0:T(8,128)(2,1)S(1)}, u32[]{:S(2)}) copy-start(bf16[1024,1024]{1,0:T(8,128)(2,1)S(1)} %collective-permute-done.3.b_ref) | copy-start | bytes 6291460
where the time goes:
time: 74.5 us; the launch traced here: 74.2 us
  Pallas kernels  60.1 us (81%)
  starting transfers between devices  10.2 us (14%)
  local copies, waits for them, and re-layouts  2.01 us (3%)
  other arithmetic  1.2 us (2%)
    pallas_call x2, Pallas kernels, mix(): pl.pallas_call(lambda *refs: mixer_kernel(len(tots), *refs), name='mixer'...  22.1 us
    pallas_call x1, Pallas kernels, project(): pl.pallas_call(project_kernel, name='project', grid=(length // rows,), in...  15.1 us
    pallas_call x1, Pallas kernels, project_out(): pl.pallas_call(output_kernel, name='output', grid_spec=pltpu.PrefetchScal...  14.2 us
    ppermute x3, starting transfers between devices, body(): lax.ppermute(value, 'sp', [(source, source + steps) for source in range(p...  8.92 us
    pallas_call x1, Pallas kernels, project_queries(): pl.pallas_call(query_kernel, name='queries', grid=(length // rows,), in_s...  8.72 us
  transfers between devices with their start and end apart: 4, of which 0 were waited for; matrix products, arithmetic and copies ran while one was open for 2% of the time, Pallas kernels for 27%

commit v1 on v0

--- a/solution.py
+++ b/solution.py
@@ -13,6 +13,7 @@
 
 ROWS = 512
 TILE = 256
+PIECE = 16
 REACH = 16
 F32 = jnp.float32
 BF16 = jnp.bfloat16
@@ -22,8 +23,8 @@
     return lax.dot_general(a, b, (dims, ((), ())), preferred_element_type=F32)
 
 
-def project_kernel(x_ref, gain_ref, wk_ref, wv_ref, wp_ref, n_ref, kv_ref, p_ref, sums_ref,
-                   tail_ref, tot_ref, wkv, total):
+def project_kernel(x_ref, gain_ref, wq_ref, wk_ref, wv_ref, wp_ref, q_ref, kv_ref, p_ref, sums_ref,
+                   tail_ref, tot_ref, wkv, total, n_ref):
     step = pl.program_id(0)
     last = pl.num_programs(0) - 1
     kw = wk_ref.shape[1]
@@ -40,11 +41,14 @@
     running = total[0:1]
     for part in range(rows // TILE):
         span = slice(part * TILE, (part + 1) * TILE)
-        x = x_ref[span].astype(F32)
-        centered = x - jnp.mean(x, axis=-1, keepdims=True)
-        variance = jnp.mean(centered * centered, axis=-1, keepdims=True)
-        normed = (centered * lax.rsqrt(variance + LN_EPS) * gain).astype(BF16)
-        n_ref[span] = normed
+        for piece in range(TILE // PIECE):
+            lines = slice(part * TILE + piece * PIECE, part * TILE + (piece + 1) * PIECE)
+            x = x_ref[lines].astype(F32)
+            centered = x - jnp.mean(x, axis=-1, keepdims=True)
+            variance = jnp.mean(centered * centered, axis=-1, keepdims=True)
+            n_ref[lines] = (centered * lax.rsqrt(variance + LN_EPS) * gain).astype(BF16)
+        normed = n_ref[span]
+        q_ref[span] = (dot(normed, wq_ref[...]) * HEAD_SIZE ** (-0.5)).astype(BF16)
         kv_ref[span] = dot(normed, wkv[...]).astype(BF16)
         pool = dot(normed, wp_ref[...]).astype(BF16)
         p_ref[span] = pool
@@ -66,9 +70,9 @@
         tail_ref[WINDOW_KEYS + REACH :] = tot
 
 
-def project(x, gain, wk, wv, wp):
+def project(x, gain, wq, wk, wv, wp):
     length, d = x.shape
-    kw, pw = wk.shape[1], wp.shape[1]
+    qw, kw, pw = wq.shape[1], wk.shape[1], wp.shape[1]
     rows = min(ROWS, length)
     whole = lambda shape: pl.BlockSpec(shape, lambda i: (0, 0))
     tail_rows = WINDOW_KEYS + 2 * REACH
@@ -79,12 +83,13 @@
         in_specs=[
             pl.BlockSpec((rows, d), lambda i: (i, 0)),
             whole((1, d)),
+            whole((d, qw)),
             whole((d, kw)),
             whole((d, kw)),
             whole((d, pw)),
         ],
         out_specs=[
-            pl.BlockSpec((rows, d), lambda i: (i, 0)),
+            pl.BlockSpec((rows, qw), lambda i: (i, 0)),
             pl.BlockSpec((rows, 2 * kw), lambda i: (i, 0)),
             pl.BlockSpec((rows, pw), lambda i: (i, 0)),
             whole((length // TILE, pw)),
@@ -92,52 +97,36 @@
             whole((REACH, pw)),
         ],
         out_shape=[
-            jax.ShapeDtypeStruct((length, d), BF16),
+            jax.ShapeDtypeStruct((length, qw), BF16),
             jax.ShapeDtypeStruct((length, 2 * kw), BF16),
             jax.ShapeDtypeStruct((length, pw), BF16),
             jax.ShapeDtypeStruct((length // TILE, pw), F32),
             jax.ShapeDtypeStruct((tail_rows, pw), BF16),
             jax.ShapeDtypeStruct((REACH, pw), BF16),
         ],
-        scratch_shapes=[pltpu.VMEM((d, 2 * kw), BF16), pltpu.VMEM((8, pw), F32)],
+        scratch_shapes=[
+            pltpu.VMEM((d, 2 * kw), BF16),
+            pltpu.VMEM((8, pw), F32),
+            pltpu.VMEM((rows, d), BF16),
+        ],
         cost_estimate=pl.CostEstimate(
-            flops=2 * length * d * (2 * kw + pw), bytes_accessed=6 * length * d, transcendentals=0
+            flops=2 * length * d * (qw + 2 * kw + pw), bytes_accessed=4 * length * d, transcendentals=0
         ),
         compiler_params=pltpu.CompilerParams(dimension_semantics=("arbitrary",)),
-    )(x, gain, wk, wv, wp)
-
-
-def query_kernel(n_ref, w_ref, q_ref):
-    q_ref[...] = (dot(n_ref[...], w_ref[...]) * HEAD_SIZE ** (-0.5)).astype(BF16)
-
-
-def project_queries(normed, wq):
-    length, d = normed.shape
-    qw = wq.shape[1]
-    rows = min(ROWS, length)
-    return pl.pallas_call(
-        query_kernel,
-        name="queries",
-        grid=(length // rows,),
-        in_specs=[
-            pl.BlockSpec((rows, d), lambda i: (i, 0)),
-            pl.BlockSpec((d, qw), lambda i: (0, 0)),
-        ],
-        out_specs=pl.BlockSpec((rows, qw), lambda i: (i, 0)),
-        out_shape=jax.ShapeDtypeStruct((length, qw), BF16),
-        cost_estimate=pl.CostEstimate(
-            flops=2 * length * d * qw, bytes_accessed=2 * length * d, transcendentals=0
-        ),
-        compiler_params=pltpu.CompilerParams(dimension_semantics=("arbitrary",)),
-    )(normed, wq)
-
-
-def mixer_kernel(further, where_ref, q_ref, kv_ref, kvp_ref, p_ref, pp_ref, sums_ref, tail_ref,
+    )(x, gain, wq, wk, wv, wp)
+
+
+def half_of(where, kept):
+    return where[0] if kept else 1 - where[0]
+
+
+def mixer_kernel(further, kept, where_ref, q_ref, kv_ref, kvp_ref, p_ref, pp_ref, sums_ref, tail_ref,
                  *refs):
     tots = refs[:further]
-    wg_ref, sink_ref, _, act_ref, log_ref = refs[further:]
+    wg_ref, sink_ref = refs[further : further + 2]
+    act_ref, log_ref = refs[-2:]
     seq_part = where_ref[1]
-    tile = where_ref[0] * pl.num_programs(0) + pl.program_id(0)
+    tile = half_of(where_ref, kept) * pl.num_programs(0) + pl.program_id(0)
     first = tile == 0
     rows, qw = q_ref.shape
     kw = kv_ref.shape[1] // 2
@@ -165,7 +154,7 @@
     )
     for slot in range(pw // GDIM):
         lanes = slice(slot * GDIM, (slot + 1) * GDIM)
-        width = jnp.left_shift(jnp.int32(2), where_ref[2] * (pw // GDIM) + slot)
+        width = jnp.left_shift(jnp.int32(2), where_ref[0] * (pw // GDIM) + slot)
         band = jnp.where((gap >= 0) & (gap < width), 1.0, 0.0).astype(BF16)
         edge = jnp.where(edge_gap < width, 1.0, 0.0).astype(BF16)
         window = dot(band, x[:, lanes])
@@ -249,7 +238,8 @@
 def mix(where, q, kv, pool, sums, tail, tots, w_group, sinks, logs, steps):
     length, qw = q.shape
     kw2, pw = kv.shape[1], pool.shape[1]
-    tile = lambda i, w: w[0] * steps + i
+    kept = logs is not None
+    tile = lambda i, w: half_of(w, kept) * steps + i
     spec = pl.BlockSpec
     heads = qw // HEAD_SIZE
     in_specs = [
@@ -265,11 +255,12 @@
     in_specs += [
         spec(w_group.shape, lambda i, w: (0, 0, 0)),
         spec(memory_space=pltpu.SMEM),
-        spec(memory_space=pl.ANY),
     ]
-    operands = (where, q, kv, kv, pool, pool, sums, tail, *tots, w_group, sinks, logs)
+    in_specs += [spec(memory_space=pl.ANY)] * kept
+    operands = (where, q, kv, kv, pool, pool, sums, tail, *tots, w_group, sinks)
+    operands += (logs,) if kept else ()
     return pl.pallas_call(
-        lambda *refs: mixer_kernel(len(tots), *refs),
+        lambda *refs: mixer_kernel(len(tots), kept, *refs),
         name="mixer",
         grid_spec=pltpu.PrefetchScalarGridSpec(
             num_scalar_prefetch=1,
@@ -284,7 +275,7 @@
             jax.ShapeDtypeStruct((steps * TILE, pw + qw), BF16),
             jax.ShapeDtypeStruct((heads, length), F32),
         ],
-        input_output_aliases={len(operands) - 1: 1},
+        input_output_aliases={len(operands) - 1: 1} if kept else {},
         cost_estimate=pl.CostEstimate(
             flops=8 * steps * TILE * (WINDOW_KEYS * qw + TILE * pw),
             bytes_accessed=6 * steps * TILE * (pw + qw),
@@ -307,7 +298,7 @@
     chunk = inner // 2
     blocks = w_out.reshape(w_out.shape[0] // chunk, chunk, d)
     spec = pl.BlockSpec
-    weight = lambda place: spec((1, chunk, width), lambda j, w: (place(w[2]), 0, j))
+    weight = lambda place: spec((1, chunk, width), lambda j, w: (place(w[0]), 0, j))
     return pl.pallas_call(
         output_kernel,
         name="output",
@@ -337,21 +328,21 @@
     length = x.shape[0]
     parts = lax.axis_size("sp")
     sp, tp = lax.axis_index("sp"), lax.axis_index("tp")
-    normed, kv, pool, sums, tail, tot = project(x, norm_gain[None, :], w_key, w_value, w_pool)
+    q, kv, pool, sums, tail, tot = project(
+        x, norm_gain[None, :], w_query, w_key, w_value, w_pool
+    )
     ahead = lambda value, steps: lax.ppermute(
         value, "sp", [(source, source + steps) for source in range(parts - steps)]
     )
     tail = ahead(tail, 1)
     tots = [ahead(tot, steps) for steps in range(2, parts)]
-    q = project_queries(normed, w_query)
     steps = length // TILE // 2
-    heads = q.shape[1] // HEAD_SIZE
-    place = lambda half: jnp.stack([half, sp, tp]).astype(jnp.int32)
-    logs = jnp.zeros((heads, length), F32)
-    sent, logs = mix(place(1 - tp), q, kv, pool, sums, tail, tots, w_group, sinks, logs, steps)
+    where = jnp.stack([tp, sp]).astype(jnp.int32)
+    shared = (where, q, kv, pool, sums, tail, tots, w_group, sinks)
+    sent, logs = mix(*shared, None, steps)
     other = lax.ppermute(sent, "tp", [(0, 1), (1, 0)])
-    own, logs = mix(place(tp), q, kv, pool, sums, tail, tots, w_group, sinks, logs, steps)
-    mixed = project_out(place(tp), own, other, w_out, 512)
+    own, logs = mix(*shared, logs, steps)
+    mixed = project_out(where, own, other, w_out, 512)
     return (mixed[None], logs[None])
 
 

time: 74.5 us -> 70.3 us (0.944)
  Pallas kernels: 60.1 us -> 55.5 us
    pallas_call x3 -> x2, Pallas kernels: 30.8 us -> 22.1 us  [mix(): pl.pallas_call(lambda *refs: mixer_kernel(len(tots), kept, *refs), name='...]
    pallas_call x1, Pallas kernels: 15.1 us -> 19.2 us  [project(): pl.pallas_call(project_kernel, name='project', grid=(length // rows,), in...]
  transfers between devices with their start and end apart: 4 -> 4, of which waited for: 0 -> 1; matrix products, arithmetic and copies ran while one was open for 2% -> 1% of each run, Pallas kernels for 27% -> 16%
where the time goes in v1:
time: 70.3 us; the launch traced here: 70 us
  Pallas kernels  55.5 us (79%)
  starting transfers between devices  10.8 us (15%)
  local copies, waits for them, and re-layouts  2 us (3%)
    pallas_call x2, Pallas kernels, mix(): pl.pallas_call(lambda *refs: mixer_kernel(len(tots), kept, *refs), name='...  22.1 us
    pallas_call x1, Pallas kernels, project(): pl.pallas_call(project_kernel, name='project', grid=(length // rows,), in...  19.2 us
    pallas_call x1, Pallas kernels, project_out(): pl.pallas_call(output_kernel, name='output', grid_spec=pltpu.PrefetchScal...  14.2 us
    ppermute x3, starting transfers between devices, body(): lax.ppermute(value, 'sp', [(source, source + steps) for source in range(p...  8.92 us
    unnamed x8, local copies, waits for them, and re-layouts  2 us
    ppermute x1, starting transfers between devices, body(): other = lax.ppermute(sent, 'tp', [(0, 1), (1, 0)])  1.85 us
  transfers between devices with their start and end apart: 4, of which 1 were waited for; matrix products, arithmetic and copies ran while one was open for 1% of the time, Pallas kernels for 16%

profile of v1, /device:TPU:1, one launch (start us, length us, event | category | flops | bytes accessed | tf_op | source)
XLA Modules:
  0.0 70.0 jit_solution(3400370353831154173)
XLA Ops:
  0.6 19.2 %project.1 = (bf16[2048,512]{1,0:T(8,128)(2,1)}, bf16[2048,256]{1,0:T(8,128)(2,1)}, bf16[2048,512]{1,0:T(8,128)(2,1)}, f32[8,512]{1,0:T(8,128)}, bf16[160,512]{1,0:T(8,128)(2,1)}, /*index=5*/bf16[16,512]{1,0:T(8,128)(2,1)}) custom-call(bf16[2048,2048]{1,0:T(8,128)(2,1)} %bitcast.13, f32[1,2048]{1,0:T(1,128)} %bitcast.14, bf16[2048,512]{1,0:T(8,128)(2,1)} %wq_ref.1, ...), custom_call_target="tpu_custom_call" | custom-call | flops 10737418240 | bytes 16777216 | tf_op jit(solution)/shard_map/project/pallas_call | solution.py:79
  19.8 4.0 %collective-permute-start = (bf16[160,512]{1,0:T(8,128)(2,1)}, bf16[160,512]{1,0:T(8,128)(2,1)S(1)}, u32[]{:S(2)}, u32[]{:S(2)}) collective-permute-start(bf16[160,512]{1,0:T(8,128)(2,1)} %get-tuple-element.16), channel_id=1, source_target_pairs={{0,8},{8,16},{16,24},{1,9},{9,17},{17,25},{2,10},{10,18},{18,26},{... | collective-permute-start | bytes 491528 | tf_op jit(solution)/shard_map/ppermute | solution.py:334
  23.9 3.3 %collective-permute-start.2 = (bf16[16,512]{1,0:T(8,128)(2,1)}, bf16[16,512]{1,0:T(8,128)(2,1)S(1)}, u32[]{:S(2)}, u32[]{:S(2)}) collective-permute-start(bf16[16,512]{1,0:T(8,128)(2,1)} %get-tuple-element.17), channel_id=1, source_target_pairs={{0,24},{1,25},{2,26},{3,27},{4,28},{5,29},{6,30},{7,31}} | collective-permute-start | bytes 49160 | tf_op jit(solution)/shard_map/ppermute | solution.py:334
  27.2 1.6 %collective-permute-start.1 = (bf16[16,512]{1,0:T(8,128)(2,1)}, bf16[16,512]{1,0:T(8,128)(2,1)S(1)}, u32[]{:S(2)}, u32[]{:S(2)}) collective-permute-start(bf16[16,512]{1,0:T(8,128)(2,1)} %get-tuple-element.17), channel_id=1, source_target_pairs={{0,16},{8,24},{1,17},{9,25},{2,18},{10,26},{3,19},{11,27},{4,20},{... | collective-permute-start | bytes 49160 | tf_op jit(solution)/shard_map/ppermute | solution.py:334
  28.8 0.7 pad_add_fusion.refs_0_.where_ref
  29.5 0.0 collective-permute-done.2.refs_9_
  29.5 0.0 copy-start.2
  29.5 0.4 collective-permute-done.1.refs_8_
  29.9 0.0 copy-start.3
  29.9 0.0 collective-permute-done.refs_7_
  29.9 0.0 copy-start.1
  29.9 0.2 copy-done.2
  30.1 0.4 copy-done.3
  30.5 0.1 copy-done.1
  30.5 11.1 %mixer.2 = (bf16[1024,1024]{1,0:T(8,128)(2,1)}, f32[8,2048]{1,0:T(8,128)}) custom-call(s32[2]{0:T(128)} %pad_add_fusion.refs_0_.where_ref, bf16[2048,512]{1,0:T(8,128)(2,1)} %get-tuple-element.12.refs_1_, bf16[2048,256]{1,0:T(8,128)(2,1)} %get-tuple-element.13.refs_2_.refs_3_, bf16[2048,256]{1,0:T(8,128)(2,1)} %get-tuple-element.13.refs_2_.refs_3_, ...), custom_call_target="tpu_custom_call" | custom-call | flops 1610612736 | bytes 6291456 | tf_op jit(solution)/shard_map/mixer/pallas_call | solution.py:262
  41.6 1.8 %collective-permute-start.3 = (bf16[1024,1024]{1,0:T(8,128)(2,1)}, bf16[1024,1024]{1,0:T(8,128)(2,1)S(1)}, u32[]{:S(2)}, u32[]{:S(2)}) collective-permute-start(bf16[1024,1024]{1,0:T(8,128)(2,1)} %get-tuple-element.20), channel_id=1, source_target_pairs={{0,1},{1,0},{2,3},{3,2},{4,5},{5,4},{6,7},{7,6},{8,9},{9,8},{10,11... | collective-permute-start | bytes 6291464 | tf_op jit(solution)/shard_map/ppermute | solution.py:343
  43.4 11.0 %mixer.3 = (bf16[1024,1024]{1,0:T(8,128)(2,1)}, f32[8,2048]{1,0:T(8,128)}) custom-call(s32[2]{0:T(128)} %pad_add_fusion.refs_0_.where_ref, bf16[2048,512]{1,0:T(8,128)(2,1)} %get-tuple-element.12.refs_1_, bf16[2048,256]{1,0:T(8,128)(2,1)} %get-tuple-element.13.refs_2_.refs_3_, ...), custom_call_target="tpu_custom_call", output_to_operand_aliasing={{1}: (12, {})} | custom-call | flops 1610612736 | bytes 6291456 | tf_op jit(solution)/shard_map/mixer/pallas_call | solution.py:262
  54.5 0.0 collective-permute-done.3.b_ref
  54.5 0.0 copy-start
  54.5 1.3 %copy-done = bf16[1024,1024]{1,0:T(8,128)(2,1)} copy-done((bf16[1024,1024]{1,0:T(8,128)(2,1)}, bf16[1024,1024]{1,0:T(8,128)(2,1)S(1)}, u32[]{:S(2)}) %copy-start) | copy-done | bytes 2097176
  55.8 14.2 %output.1 = bf16[1024,2048]{1,0:T(8,128)(2,1)} custom-call(s32[2]{0:T(128)} %pad_add_fusion.refs_0_.where_ref, bf16[1024,1024]{1,0:T(8,128)(2,1)} %get-tuple-element.19.a_ref, bf16[1024,1024]{1,0:T(8,128)(2,1)} %copy-done, bf16[4,512,2048]{2,1,0:T(8,128)(2,1)} %bitcast.7, bf16[4,512,2048]{2,1,0:T(8,128)(2,1)} %bitcast.8, bf16[4,512,2048]{2,1,0:T(8,128)(2,1)} %bitcast.9, ...), custom_call_target="tpu_custom_call" | custom-call | flops 8589934592 | bytes 12582912 | tf_op jit(solution)/shard_map/output/pallas_call | solution.py:302
Async XLA Ops:
  19.8 10.0 %collective-permute-start = (bf16[160,512]{1,0:T(8,128)(2,1)}, bf16[160,512]{1,0:T(8,128)(2,1)S(1)}, u32[]{:S(2)}, u32[]{:S(2)}) collective-permute-start(bf16[160,512]{1,0:T(8,128)(2,1)} %get-tuple-element.16), channel_id=1, source_target_pairs={{0,8},{8,16},{16,24},{1,9},{9,17},{17,25},{2,10},{10,18},{18,26},{... | collective-permute-start | bytes 491528 | tf_op jit(solution)/shard_map/ppermute | solution.py:334
  23.9 5.6 %collective-permute-start.2 = (bf16[16,512]{1,0:T(8,128)(2,1)}, bf16[16,512]{1,0:T(8,128)(2,1)S(1)}, u32[]{:S(2)}, u32[]{:S(2)}) collective-permute-start(bf16[16,512]{1,0:T(8,128)(2,1)} %get-tuple-element.17), channel_id=1, source_target_pairs={{0,24},{1,25},{2,26},{3,27},{4,28},{5,29},{6,30},{7,31}} | collective-permute-start | bytes 49160 | tf_op jit(solution)/shard_map/ppermute | solution.py:334
  27.2 2.6 %collective-permute-start.1 = (bf16[16,512]{1,0:T(8,128)(2,1)}, bf16[16,512]{1,0:T(8,128)(2,1)S(1)}, u32[]{:S(2)}, u32[]{:S(2)}) collective-permute-start(bf16[16,512]{1,0:T(8,128)(2,1)} %get-tuple-element.17), channel_id=1, source_target_pairs={{0,16},{8,24},{1,17},{9,25},{2,18},{10,26},{3,19},{11,27},{4,20},{... | collective-permute-start | bytes 49160 | tf_op jit(solution)/shard_map/ppermute | solution.py:334
  29.5 0.6 copy-start.2
  29.9 0.6 copy-start.3
  29.9 0.7 copy-start.1
  41.6 12.9 %collective-permute-start.3 = (bf16[1024,1024]{1,0:T(8,128)(2,1)}, bf16[1024,1024]{1,0:T(8,128)(2,1)S(1)}, u32[]{:S(2)}, u32[]{:S(2)}) collective-permute-start(bf16[1024,1024]{1,0:T(8,128)(2,1)} %get-tuple-element.20), channel_id=1, source_target_pairs={{0,1},{1,0},{2,3},{3,2},{4,5},{5,4},{6,7},{7,6},{8,9},{9,8},{10,11... | collective-permute-start | bytes 6291464 | tf_op jit(solution)/shard_map/ppermute | solution.py:343
  54.5 1.3 %copy-start = (bf16[1024,1024]{1,0:T(8,128)(2,1)}, bf16[1024,1024]{1,0:T(8,128)(2,1)S(1)}, u32[]{:S(2)}) copy-start(bf16[1024,1024]{1,0:T(8,128)(2,1)S(1)} %collective-permute-done.3.b_ref) | copy-start | bytes 6291460
